TPU v7x, 256 devices: a whole 4x4x8 slice. The times are simulated.
256 devices in a mesh: ep: 64 (over z, y, core), tp: 4 (over x).
Axes of the slice: x: 4, y: 4, z: 8, core: 2. Of those that a mesh axis runs over, the one named last changes fastest.
Arguments:
- tokens: bfloat16 [49152, 2048], P('ep', 'tp')
- norm_gain: float32 [2048], P('tp'), may hold values from 0.1 to 1.9
- routing: int32 [49152, 2], P('ep'), may hold values from 0 to 63, as said below
- route_weight: float32 [49152, 2], P('ep'), may hold values from 0.2 to 1
- w_gate: bfloat16 [64, 2048, 512], P('ep', 'tp'), may hold values from -0.125 to 0.125
- w_up: bfloat16 [64, 2048, 512], P('ep', 'tp'), may hold values from -0.125 to 0.125
- w_down: bfloat16 [64, 512, 2048], P('ep', None, 'tp'), may hold values from -0.25 to 0.25
- w_branch_in: bfloat16 [2048, 1024], P('ep', 'tp'), may hold values from -0.125 to 0.125
- w_branch_out: bfloat16 [1024, 2048], P('tp', 'ep'), may hold values from -0.1875 to 0.1875
- branch_gate: float32 [2048], P('tp'), may hold values from -3 to 3
Outputs:
- mixed: bfloat16 [49152, 2048], P('ep', 'tp')
Inputs may be any that keep to these rules, and one draw needn't show every extreme that they name: `routing`: each row names two different experts of the same group; expert e belongs to group e // 16. Among the rows of one device (aligned blocks of 768 rows) no expert is named more than 48 times, and in every block all experts of one group are named exactly 48 times.
All inputs are finite; a program needn't handle non-finite values.
Results may differ from a plain program's by a relative error of at most 0.0069.
Values may be sent and summed in bfloat16 or wider, within the bound.
A program may use at most 128 MiB of HBM per device.

v0:
```python
import jax
import jax.numpy as jnp
from jax import lax
from jax.sharding import PartitionSpec as P

GROUPS = 4
epsilon = 1e-06


def sent_to_all(value, axis):
    size = lax.axis_size(axis)
    return lax.all_to_all(
        jnp.broadcast_to(value[None], (size, *value.shape)), axis, 0, 0, tiled=True
    )


def taken_together(value, axis):
    return sent_to_all(value, axis).sum(axis=0)


def gather_turned(arrays, axis, dims):
    turned = [jnp.moveaxis(a, dim, 0) for a, dim in zip(arrays, dims)]
    both = jnp.concatenate([t.reshape(len(t), -1) for t in turned], axis=1)
    filled, at, gathered = (lax.all_gather(both, axis, axis=0, tiled=True), 0, [])
    for t, dim in zip(turned, dims):
        share = filled[:, at : at + t[0].size].reshape(-1, *t.shape[1:])
        gathered.append(jnp.moveaxis(share, 0, dim))
        at += t[0].size
    return tuple(gathered)


def send_back(result):
    return lax.all_to_all(result, "ep", split_axis=0, concat_axis=0, tiled=True)


def body(
    tokens,
    norm_gain,
    routing,
    route_weight,
    w_gate,
    w_up,
    w_down,
    w_branch_in,
    w_branch_out,
    branch_gate,
):
    token_count, quarter = tokens.shape
    full_width = quarter * lax.axis_size("tp")
    floats = tokens.astype(jnp.float32)
    squares = taken_together(jnp.sum(floats * floats, axis=1), "tp")
    normed = (floats * lax.rsqrt(squares[:, None] / full_width + epsilon) * norm_gain).astype(
        jnp.bfloat16
    )
    expert_count = lax.axis_size("ep") * w_gate.shape[0]
    capacity = token_count // (expert_count // GROUPS)
    flat_ids = routing.reshape(-1)
    one_hot = (flat_ids[:, None] == jnp.arange(expert_count, dtype=jnp.int32)[None, :]).astype(
        jnp.int32
    )
    before = jnp.cumsum(one_hot, axis=0) - one_hot
    position = flat_ids * capacity + jnp.sum(before * one_hot, axis=1)
    copies = jnp.repeat(normed, 2, axis=0)
    buffer = jnp.zeros((expert_count * capacity, quarter), jnp.bfloat16).at[position].set(copies)
    buffer = buffer.reshape(expert_count, capacity, quarter)
    gate_whole, up_whole, down_whole = (
        lax.all_gather(w_gate[0], "tp", axis=0, tiled=True),
        lax.all_gather(w_up[0], "tp", axis=0, tiled=True),
        lax.all_gather(w_down[0], "tp", axis=1, tiled=True),
    )
    row_split = lax.all_to_all(
        lax.all_to_all(buffer, "ep", split_axis=0, concat_axis=0, tiled=True),
        "tp",
        split_axis=0,
        concat_axis=2,
        tiled=True,
    )
    slot_rows = row_split.reshape(-1, row_split.shape[2])
    gate_sum = jnp.dot(slot_rows, gate_whole, preferred_element_type=jnp.float32)
    up_sum = jnp.dot(slot_rows, up_whole, preferred_element_type=jnp.float32)
    hidden = (jax.nn.silu(gate_sum) * up_sum).astype(jnp.bfloat16)
    result = jnp.dot(hidden, down_whole, preferred_element_type=jnp.float32).astype(jnp.bfloat16)
    feature_split = lax.all_to_all(
        result.reshape(row_split.shape), "tp", split_axis=2, concat_axis=0, tiled=True
    )
    returned = send_back(feature_split)
    picked = returned.reshape(expert_count * capacity, quarter)[position].reshape(
        token_count, 2, quarter
    )
    routed = jnp.sum(picked.astype(jnp.float32) * route_weight[:, :, None], axis=1)
    branch_tokens = lax.all_to_all(normed, "tp", split_axis=0, concat_axis=1, tiled=True)
    in_cols, out_rows = gather_turned((w_branch_in, w_branch_out), "tp", (1, 0))
    in_whole, out_whole = gather_turned((in_cols, out_rows), "ep", (0, 1))
    branch_hidden = jax.nn.silu(
        jnp.dot(branch_tokens, in_whole, preferred_element_type=jnp.float32)
    ).astype(jnp.bfloat16)
    branch_local = jnp.dot(branch_hidden, out_whole, preferred_element_type=jnp.float32).astype(
        jnp.bfloat16
    )
    branch = lax.all_to_all(branch_local, "tp", split_axis=1, concat_axis=0, tiled=True)
    return (routed + jax.nn.sigmoid(branch_gate) * branch.astype(jnp.float32)).astype(jnp.bfloat16)


def solution(mesh):
    return jax.shard_map(
        body,
        mesh=mesh,
        in_specs=(
            P("ep", "tp"),
            P("tp"),
            P("ep", None),
            P("ep", None),
            P("ep", "tp", None),
            P("ep", "tp", None),
            P("ep", None, "tp"),
            P("ep", "tp"),
            P("tp", "ep"),
            P("tp"),
        ),
        out_specs=P("ep", "tp"),
        check_vma=False,
    )
```

profile of v0, /device:TPU:2, one launch (start us, length us, event | category | flops | bytes accessed | tf_op | source)
XLA Modules:
  0.0 391.7 jit_solution(14819414351238019944)
XLA Ops:
  6.5 0.7 all-gather.10.cloned.1.call-update
  7.3 0.7 all-gather.12.cloned.1.call-update
  8.0 1.4 fusion.12
  9.4 0.6 broadcast_in_dim.7
  10.0 5.5 %all-to-all-start = ((f32[4,1,768]{2,1,0:T(1,128)}), f32[4,1,768]{2,1,0:T(1,128)S(1)}, u32[]{:S(2)}, u32[]{:S(2)}) async-start(f32[4,1,768]{2,1,0:T(1,128)} %broadcast_in_dim.7), calls=%async_computation | async-start | bytes 24576 | tf_op jit(solution)/shard_map/all_to_all | solution.py:12
  15.4 0.7 all-gather.14.cloned.1.call-update
  16.2 0.2 copy.56
  16.4 0.2 eq.29
  16.6 0.2 eq.25
  16.9 18.1 %reduce-window.6 = s32[64,12,128]{2,1,0:T(8,128)S(1)} reduce-window(s32[64,12,128]{2,1,0:T(8,128)S(1)} %fusion.27, s32[]{:T(128)} %constant.6.clone.1), window={size=1x1x128 pad=0_0x0_0x127_0}, to_apply=%region_0.0 | reduce-window | flops 12484608 | bytes 786436 | tf_op jit(solution)/shard_map/reduce-window
  35.0 0.2 slice.26
  35.2 0.3 copy.58
  35.6 0.2 copy.55
  35.8 0.3 mul.67
  36.1 0.2 broadcast_add_fusion
  36.3 0.2 fusion.30
  36.6 0.2 fusion.14
  36.8 0.9 copy-done
  37.7 0.8 broadcast_in_dim.8
  38.5 0.6 reshape.110
  39.2 9.5 %scatter_custom_fusion = bf16[3072,512]{1,0:T(8,128)(2,1)} fusion(s32[1536]{0:T(1024)S(1)} %fusion.32, bf16[1536,512]{1,0:T(8,128)(2,1)S(1)} %reshape.110, bf16[]{:T(256)} %constant.8.clone.1), kind=kCustom, calls=%fused_computation.23 | custom fusion | bytes 3145730 | tf_op jit(solution)/shard_map/scatter | solution.py:64
  48.7 11.6 %all-to-all-start.1 = ((bf16[64,48,512]{2,1,0:T(8,128)(2,1)}), bf16[64,48,512]{2,1,0:T(8,128)(2,1)S(1)}, u32[]{:S(2)}, u32[]{:S(2)}) async-start(bf16[64,48,512]{2,1,0:T(8,128)(2,1)} %bitcast.74), calls=%async_computation.1 | async-start | bytes 6291456 | tf_op jit(solution)/shard_map/all_to_all | solution.py:72
  60.4 12.7 %all_gather.18 = bf16[1024,64]{0,1:T(8,128)(2,1)S(1)} all-gather(bf16[256,64]{0,1:T(8,128)(2,1)S(1)} %pad_maximum_fusion.1), channel_id=1, replica_groups=mesh['ep'=64,'tp'=4] {'tp'}, dimensions={0}, use_global_device_ids=true | all-gather | bytes 163840 | tf_op jit(solution)/shard_map/all_gather | solution.py:24
  73.1 0.7 pad_maximum_fusion
  73.7 60.4 %all-to-all-done.1 = bf16[64,48,512]{2,1,0:T(8,128)(2,1)S(1)} async-done(((bf16[64,48,512]{2,1,0:T(8,128)(2,1)}), bf16[64,48,512]{2,1,0:T(8,128)(2,1)S(1)}, u32[]{:S(2)}, u32[]{:S(2)}) %all-to-all-start.1) | async-done | bytes 3145760 | tf_op jit(solution)/shard_map/all_to_all | solution.py:72
  134.2 39.5 %all_to_all.81 = bf16[64,48,512]{2,1,0:T(8,128)(2,1)S(1)} all-to-all(bf16[64,48,512]{2,1,0:T(8,128)(2,1)S(1)} %all-to-all-done.1), channel_id=1, replica_groups=mesh['ep'=64,'tp'=4] {'tp'}, dimensions={0} | all-to-all | bytes 6291456 | tf_op jit(solution)/shard_map/all_to_all | solution.py:71
  173.6 2.6 copy.61
  176.3 1.0 copy.71
  177.3 4.6 %fusion.10 = f32[768,512]{1,0:T(8,128)} fusion(bf16[768,2048]{1,0:T(8,128)(2,1)S(1)} %bitcast.79, bf16[1,2048,512]{2,1,0:T(8,128)(2,1)} %all-gather.10.cloned.1.call-done), kind=kOutput, calls=%fused_computation.12 | convolution fusion | flops 1610612736 | bytes 6815744 | tf_op jit(solution)/shard_map/dot_general | solution.py:79
  182.0 7.9 %convolution_convert_fusion = bf16[768,2048]{1,0:T(8,128)(2,1)} fusion(bf16[1,512,2048]{2,1,0:T(8,128)(2,1)} %all-gather.14.cloned.1.call-done, f32[768,512]{1,0:T(8,128)} %fusion.10, bf16[768,2048]{1,0:T(8,128)(2,1)S(1)} %bitcast.80, bf16[1,2048,512]{2,1,0:T(8,128)(2,1)} %all-gather.12.cloned.1.call-done), kind=kOutput, calls=%fused_computation.6 | convolution fusion | flops 3225157632 | bytes 12058624 | tf_op jit(solution)/shard_map/dot_general | solution.py:82
  189.9 10.5 %copy.62 = bf16[16,48,2048]{1,0,2:T(8,128)(2,1)} copy(bf16[16,48,2048]{2,1,0:T(8,128)(2,1)} %bitcast.82) | data formatting | bytes 6291456 | tf_op jit(solution)/shard_map/reshape | solution.py:84
  200.4 14.8 %reshape.120 = bf16[4,2,196608]{2,1,0:T(2,128)(2,1)} reshape(bf16[2048,16,48]{2,1,0:T(8,128)(2,1)} %bitcast.72) | data formatting | bytes 6291456
  215.2 38.8 %all_to_all.82 = bf16[4,2,196608]{2,1,0:T(2,128)(2,1)S(1)} all-to-all(bf16[4,2,196608]{2,1,0:T(2,128)(2,1)} %reshape.120), channel_id=1, replica_groups=mesh['ep'=64,'tp'=4] {'tp'}, dimensions={0} | all-to-all | bytes 6291456 | tf_op jit(solution)/shard_map/all_to_all | solution.py:83
  254.0 5.6 %all-to-all-start.5 = ((bf16[4,192,512]{2,1,0:T(8,128)(2,1)}), bf16[4,192,512]{2,1,0:T(8,128)(2,1)}, u32[]{:S(2)}, u32[]{:S(2)}) async-start(bf16[4,192,512]{2,1,0:T(8,128)(2,1)} %bitcast.78), calls=%async_computation.5 | async-start | bytes 1572864 | tf_op jit(solution)/shard_map/all_to_all | solution.py:91
  259.6 9.9 %reshape.121 = bf16[2048,16,48]{2,1,0:T(8,128)(2,1)} reshape(bf16[4,2,196608]{2,1,0:T(2,128)(2,1)S(1)} %all_to_all.82) | data formatting | bytes 6291456
  269.5 9.5 %copy.63 = bf16[4,16,48,512]{3,2,1,0:T(8,128)(2,1)} copy(bf16[4,16,48,512]{2,1,3,0:T(8,128)(2,1)} %bitcast.73) | data formatting | bytes 6291456 | tf_op jit(solution)/shard_map/all_to_all | solution.py:83
  279.1 9.2 %all-to-all-start.4 = ((bf16[64,48,512]{2,1,0:T(8,128)(2,1)}), bf16[64,48,512]{2,1,0:T(8,128)(2,1)S(1)}, u32[]{:S(2)}, u32[]{:S(2)}) async-start(bf16[64,48,512]{2,1,0:T(8,128)(2,1)} %bitcast.77), calls=%async_computation.4 | async-start | bytes 6291456 | tf_op jit(solution)/shard_map/all_to_all | solution.py:33
  288.3 2.1 copy.69
  290.4 7.0 %fusion.4 = bf16[192,2048]{1,0:T(8,128)(2,1)} fusion(bf16[2048,2048]{1,0:T(8,128)(2,1)} %all-gather.8.cloned.1.call-done, bf16[192,2048]{1,0:T(8,128)(2,1)} %bitcast.84), kind=kOutput, calls=%fused_computation.8 | convolution fusion | flops 1611988992 | bytes 9961472 | tf_op jit(solution)/shard_map/dot_general | solution.py:97
  297.4 2.1 copy.74
  299.5 62.6 %all-to-all-done.4 = bf16[64,48,512]{2,1,0:T(8,128)(2,1)S(1)} async-done(((bf16[64,48,512]{2,1,0:T(8,128)(2,1)}), bf16[64,48,512]{2,1,0:T(8,128)(2,1)S(1)}, u32[]{:S(2)}, u32[]{:S(2)}) %all-to-all-start.4) | async-done | bytes 3145760 | tf_op jit(solution)/shard_map/all_to_all | solution.py:33
  362.1 4.8 %all-to-all-start.6 = ((bf16[192,4,512]{2,0,1:T(8,128)(2,1)}), bf16[192,4,512]{2,0,1:T(8,128)(2,1)}, u32[]{:S(2)}, u32[]{:S(2)}) async-start(bf16[192,4,512]{2,0,1:T(8,128)(2,1)} %bitcast.81), calls=%async_computation.6 | async-start | bytes 1572864 | tf_op jit(solution)/shard_map/all_to_all | solution.py:100
  366.9 0.6 add_divide_fusion
  367.5 0.2 copy.64
  367.7 5.4 %gather_fusion = bf16[1536,512]{1,0:T(8,128)(2,1)} fusion(bf16[3072,512]{1,0:T(8,128)(2,1)S(1)} %bitcast.71, s32[2048]{0:T(1024)S(1)} %pad_clamp_fusion), kind=kCustom, calls=%fused_computation | custom fusion | bytes 3151872 | tf_op jit(solution)/shard_map/gather | solution.py:87
  373.1 3.4 reshape.96
  376.5 5.9 %multiply_reduce_fusion = f32[768,512]{1,0:T(8,128)} fusion(f32[768,2,512]{2,1,0:T(2,128)S(1)} %reshape.96, f32[768,2]{1,0:T(8,128)S(1)} %copy.64), kind=kLoop, calls=%fused_computation.7 | loop fusion | flops 1179648 | bytes 4724736 | tf_op jit(solution)/shard_map/reduce_sum | solution.py:90
  382.4 2.7 fusion.16
  (39 shorter events, 0.4 us)
Async XLA Ops:
  6.5 9.6 %copy-start.2 = (s32[768,2]{0,1:T(2,128)S(1)}, s32[768,2]{0,1:T(2,128)}, u32[]{:S(2)}) copy-start(s32[768,2]{0,1:T(2,128)} %param.12) | copy-start | bytes 18436
  6.5 170.8 %all-gather.10.cloned.1.call-start = ((), (), s32[]{:S(2)}) async-start(), calls=%async_computation.8 | async-start | bytes 2621440 | tf_op jit(solution)/shard_map/all_gather | solution.py:67
  7.3 174.7 %all-gather.12.cloned.1.call-start = ((), (), s32[]{:S(2)}) async-start(), calls=%async_computation.9 | async-start | bytes 2621440 | tf_op jit(solution)/shard_map/all_gather | solution.py:68
  10.0 26.5 %all-to-all-start = ((f32[4,1,768]{2,1,0:T(1,128)}), f32[4,1,768]{2,1,0:T(1,128)S(1)}, u32[]{:S(2)}, u32[]{:S(2)}) async-start(f32[4,1,768]{2,1,0:T(1,128)} %broadcast_in_dim.7), calls=%async_computation | async-start | bytes 24576 | tf_op jit(solution)/shard_map/all_to_all | solution.py:12
  15.4 166.5 %all-gather.14.cloned.1.call-start = ((), (), s32[]{:S(2)}) async-start(), calls=%async_computation.10 | async-start | bytes 2621440 | tf_op jit(solution)/shard_map/all_gather | solution.py:69
  35.0 1.6 copy-start.1
  35.0 1.6 copy-start.7
  36.8 0.9 copy-start
  48.7 11.7 %copy-start.3 = (bf16[256,32]{0,1:T(8,128)(2,1)S(1)}, bf16[256,32]{0,1:T(8,128)(2,1)}, u32[]{:S(2)}) copy-start(bf16[256,32]{0,1:T(8,128)(2,1)} %param.18) | copy-start | bytes 49156
  48.7 11.7 %copy-start.4 = (bf16[32,256]{1,0:T(8,128)(2,1)S(1)}, bf16[32,256]{1,0:T(8,128)(2,1)}, u32[]{:S(2)}) copy-start(bf16[32,256]{1,0:T(8,128)(2,1)} %param.17) | copy-start | bytes 49156
  48.7 85.5 %all-to-all-start.1 = ((bf16[64,48,512]{2,1,0:T(8,128)(2,1)}), bf16[64,48,512]{2,1,0:T(8,128)(2,1)S(1)}, u32[]{:S(2)}, u32[]{:S(2)}) async-start(bf16[64,48,512]{2,1,0:T(8,128)(2,1)} %bitcast.74), calls=%async_computation.1 | async-start | bytes 6291456 | tf_op jit(solution)/shard_map/all_to_all | solution.py:72
  60.3 230.1 %all-gather.8.cloned.1.call-start = ((), (), s32[]{:S(2)}) async-start(), calls=%async_computation.7 | async-start | bytes 8519680 | tf_op jit(solution)/shard_map/all_gather | solution.py:24
  254.0 25.0 %all-to-all-start.5 = ((bf16[4,192,512]{2,1,0:T(8,128)(2,1)}), bf16[4,192,512]{2,1,0:T(8,128)(2,1)}, u32[]{:S(2)}, u32[]{:S(2)}) async-start(bf16[4,192,512]{2,1,0:T(8,128)(2,1)} %bitcast.78), calls=%async_computation.5 | async-start | bytes 1572864 | tf_op jit(solution)/shard_map/all_to_all | solution.py:91
  279.1 83.1 %all-to-all-start.4 = ((bf16[64,48,512]{2,1,0:T(8,128)(2,1)}), bf16[64,48,512]{2,1,0:T(8,128)(2,1)S(1)}, u32[]{:S(2)}, u32[]{:S(2)}) async-start(bf16[64,48,512]{2,1,0:T(8,128)(2,1)} %bitcast.77), calls=%async_computation.4 | async-start | bytes 6291456 | tf_op jit(solution)/shard_map/all_to_all | solution.py:33
  297.4 69.5 %copy-start.8 = (f32[512]{0:T(512)S(1)}, f32[512]{0:T(512)}, u32[]{:S(2)}) copy-start(f32[512]{0:T(512)} %param.19) | copy-start | bytes 6148
  297.4 70.1 %copy-start.6 = (f32[768,2]{0,1:T(2,128)S(1)}, f32[768,2]{0,1:T(2,128)}, u32[]{:S(2)}) copy-start(f32[768,2]{0,1:T(2,128)} %param.13) | copy-start | bytes 18436
  362.1 20.3 %all-to-all-start.6 = ((bf16[192,4,512]{2,0,1:T(8,128)(2,1)}), bf16[192,4,512]{2,0,1:T(8,128)(2,1)}, u32[]{:S(2)}, u32[]{:S(2)}) async-start(bf16[192,4,512]{2,0,1:T(8,128)(2,1)} %bitcast.81), calls=%async_computation.6 | async-start | bytes 1572864 | tf_op jit(solution)/shard_map/all_to_all | solution.py:100
  376.5 5.9 %copy-start.5 = (f32[512]{0:T(512)S(1)}, f32[512]{0:T(512)}, u32[]{:S(2)}) copy-start(f32[512]{0:T(512)} %add_divide_fusion) | copy-start | bytes 6148
Sparse Core Ops, SparseCore 0:
  9.1 35.3 all-gather.9
  46.3 34.3 all-gather.11
  82.6 33.3 all-gather.13
  118.6 83.9 all-gather.7
where the time goes:
time: 393 us; the launch traced here: 392 us
  waiting for transfers between devices  125 us (32%)
  blocking collectives  91 us (23%)
  local copies, waits for them, and re-layouts  75.8 us (19%)
  starting transfers between devices  36.7 us (9%)
  other arithmetic  30.1 us (8%)
  matrix products  19.5 us (5%)
  between operations  13.4 us (3%)
    all_to_all x1, waiting for transfers between devices, send_back(): return lax.all_to_all(result, 'ep', split_axis=0, concat_axis=0, tiled=True)  62.6 us
    all_to_all x1, waiting for transfers between devices, body(): lax.all_to_all(buffer, 'ep', split_axis=0, concat_axis=0, tiled=True)  60.4 us
    all_to_all x1, blocking collectives, body(): lax.all_to_all(lax.all_to_all(buffer, 'ep', split_axis=0, concat_axis=0,...  39.5 us
    all_to_all x1, blocking collectives, body(): lax.all_to_all(result.reshape(row_split.shape), 'tp', split_axis=2, conca...  38.8 us
    unnamed x23, local copies, waits for them, and re-layouts  27 us
    another operation x3, other arithmetic  18.4 us
    all_gather x1, blocking collectives, gather_turned(): lax.all_gather(both, axis, axis=0, tiled=True)  12.7 us
    all_to_all x1, starting transfers between devices, body(): lax.all_to_all(buffer, 'ep', split_axis=0, concat_axis=0, tiled=True)  11.6 us
  transfers between devices with their start and end apart: 9, of which 2 were waited for; matrix products, arithmetic and copies ran while one was open for 31% of the time, Pallas kernels for 0%

commit v1 on v0

--- a/solution.py
+++ b/solution.py
@@ -45,6 +45,32 @@
     w_branch_out,
     branch_gate,
 ):
+
+    def process_flows_over_axis(mat, at_axis, which_dim):
+        link_axis = "tp"
+        arr_out = lax.axis_size(link_axis)
+        e_now = lax.axis_index(link_axis)
+        s_next, mid_arr = (arr_out, e_now)
+        part_now = list(mat.shape)
+        long_array = mat.shape[at_axis] // s_next
+        part_now[at_axis] = long_array
+        y2 = part_now[which_dim]
+        part_now[which_dim] = y2 * s_next
+        r1 = jnp.zeros(part_now, mat.dtype)
+        for it in range(s_next):
+            all_values = lax.dynamic_slice_in_dim(
+                mat, (mid_arr ^ it) * long_array, long_array, axis=at_axis
+            )
+            if it:
+                extra = range(s_next)
+                z2 = map(lambda hop_no: (hop_no, hop_no ^ it), extra)
+                work_now = list(z2)
+                all_values = lax.ppermute(all_values, link_axis, work_now)
+            r1 = lax.dynamic_update_slice_in_dim(
+                r1, all_values, (mid_arr ^ it) * y2, axis=which_dim
+            )
+        return r1
+
     token_count, quarter = tokens.shape
     full_width = quarter * lax.axis_size("tp")
     floats = tokens.astype(jnp.float32)
@@ -80,9 +106,7 @@
     up_sum = jnp.dot(slot_rows, up_whole, preferred_element_type=jnp.float32)
     hidden = (jax.nn.silu(gate_sum) * up_sum).astype(jnp.bfloat16)
     result = jnp.dot(hidden, down_whole, preferred_element_type=jnp.float32).astype(jnp.bfloat16)
-    feature_split = lax.all_to_all(
-        result.reshape(row_split.shape), "tp", split_axis=2, concat_axis=0, tiled=True
-    )
+    feature_split = process_flows_over_axis(result.reshape(row_split.shape), 2, 0)
     returned = send_back(feature_split)
     picked = returned.reshape(expert_count * capacity, quarter)[position].reshape(
         token_count, 2, quarter

time: 393 us -> 367 us (0.934)
  blocking collectives: 91 us -> 12.6 us
  waiting for transfers between devices: 125 us -> 202 us
  local copies, waits for them, and re-layouts: 75.8 us -> 39.7 us
  starting transfers between devices: 36.7 us -> 50.1 us
    all_to_all x2 -> x0, blocking collectives: 78.3 us -> none  [the longest x1 39.5 us: body(): lax.all_to_all(lax.all_to_all(buffer, 'ep', split_axis=0, concat_axis=0,...]
    all_to_all x0 -> x1, waiting for transfers between devices: none -> 34.6 us  [body(): lax.all_to_all(lax.all_to_all(buffer, 'ep', split_axis=0, concat_axis=0,...]
    ppermute x0 -> x3, waiting for transfers between devices: none -> 26.7 us  [process_flows_over_axis(): all_values = lax.ppermute(all_values, link_axis, work_now)]
    unnamed x23 -> x25, local copies, waits for them, and re-layouts: 27 us -> 5.53 us
    all_to_all x1, waiting for transfers between devices: 60.4 us -> 74.7 us  [body(): lax.all_to_all(buffer, 'ep', split_axis=0, concat_axis=0, tiled=True)]
    reshape x1 -> x0, local copies, waits for them, and re-layouts: 10.5 us -> none  [body(): result.reshape(row_split.shape)]
    all_to_all x1 -> x0, local copies, waits for them, and re-layouts: 9.54 us -> none  [body(): lax.all_to_all(result.reshape(row_split.shape), 'tp', split_axis=2, conca...]
    all_to_all x0 -> x1, starting transfers between devices: none -> 4.56 us  [body(): lax.all_to_all(lax.all_to_all(buffer, 'ep', split_axis=0, concat_axis=0,...]
  transfers between devices with their start and end apart: 9 -> 13, of which waited for: 2 -> 7; matrix products, arithmetic and copies ran while one was open for 31% -> 22% of each run, Pallas kernels for 0% -> 0%
where the time goes in v1:
time: 367 us; the launch traced here: 366 us
  waiting for transfers between devices  202 us (55%)
  starting transfers between devices  50.1 us (14%)
  local copies, waits for them, and re-layouts  39.7 us (11%)
  other arithmetic  29.1 us (8%)
  matrix products  19.6 us (5%)
  between operations  13.4 us (4%)
  blocking collectives  12.6 us (3%)
    all_to_all x1, waiting for transfers between devices, body(): lax.all_to_all(buffer, 'ep', split_axis=0, concat_axis=0, tiled=True)  74.7 us
    all_to_all x1, waiting for transfers between devices, send_back(): return lax.all_to_all(result, 'ep', split_axis=0, concat_axis=0, tiled=True)  62.4 us
    all_to_all x1, waiting for transfers between devices, body(): lax.all_to_all(lax.all_to_all(buffer, 'ep', split_axis=0, concat_axis=0,...  34.6 us
    ppermute x3, waiting for transfers between devices, process_flows_over_axis(): all_values = lax.ppermute(all_values, link_axis, work_now)  26.7 us
    another operation x3, other arithmetic  18.4 us
    all_gather x1, blocking collectives, gather_turned(): lax.all_gather(both, axis, axis=0, tiled=True)  12.6 us
    all_to_all x1, starting transfers between devices, body(): lax.all_to_all(buffer, 'ep', split_axis=0, concat_axis=0, tiled=True)  11.6 us
    all_to_all x1, starting transfers between devices, send_back(): return lax.all_to_all(result, 'ep', split_axis=0, concat_axis=0, tiled=True)  9.61 us
  transfers between devices with their start and end apart: 13, of which 7 were waited for; matrix products, arithmetic and copies ran while one was open for 22% of the time, Pallas kernels for 0%

profile of v1, /device:TPU:2, one launch (start us, length us, event | category | flops | bytes accessed | tf_op | source)
XLA Modules:
  0.0 366.3 jit_solution(14479553542730330553)
XLA Ops:
  6.5 0.7 all-gather.10.cloned.1.call-update
  7.3 0.7 all-gather.14.cloned.1.call-update
  8.1 0.7 all-gather.12.cloned.1.call-update
  9.0 0.6 broadcast_in_dim.10
  9.6 5.5 %all-to-all-start = ((f32[4,1,768]{2,1,0:T(1,128)}), f32[4,1,768]{2,1,0:T(1,128)S(1)}, u32[]{:S(2)}, u32[]{:S(2)}) async-start(f32[4,1,768]{2,1,0:T(1,128)} %broadcast_in_dim.10), calls=%async_computation | async-start | bytes 24576 | tf_op jit(solution)/shard_map/all_to_all | solution.py:12
  15.9 0.3 mul.91
  16.2 18.1 %reduce-window.6 = s32[64,12,128]{2,1,0:T(8,128)S(1)} reduce-window(s32[64,12,128]{2,1,0:T(8,128)S(1)} %fusion.27, s32[]{:T(128)} %constant.18.clone.1), window={size=1x1x128 pad=0_0x0_0x127_0}, to_apply=%region_0.0 | reduce-window | flops 12484608 | bytes 786436 | tf_op jit(solution)/shard_map/reduce-window
  34.6 0.3 copy.51
  35.4 12.6 %all_gather.18 = bf16[1024,64]{0,1:T(8,128)(2,1)S(1)} all-gather(bf16[256,64]{0,1:T(8,128)(2,1)S(1)} %pad_maximum_fusion.1), channel_id=1, replica_groups=mesh['ep'=64,'tp'=4] {'tp'}, dimensions={0}, use_global_device_ids=true | all-gather | bytes 163840 | tf_op jit(solution)/shard_map/all_gather | solution.py:24
  48.1 0.2 fusion.14
  48.4 0.9 copy-done.1
  49.2 0.8 broadcast_in_dim.11
  50.1 0.6 reshape.110
  50.7 9.5 %scatter_custom_fusion = bf16[3072,512]{1,0:T(8,128)(2,1)} fusion(s32[1536]{0:T(1024)S(1)} %fusion.32, bf16[1536,512]{1,0:T(8,128)(2,1)S(1)} %reshape.110, bf16[]{:T(256)} %constant.16.clone.1), kind=kCustom, calls=%fused_computation.23 | custom fusion | bytes 3145730 | tf_op jit(solution)/shard_map/scatter | solution.py:90
  60.2 11.6 %all-to-all-start.1 = ((bf16[64,48,512]{2,1,0:T(8,128)(2,1)}), bf16[64,48,512]{2,1,0:T(8,128)(2,1)}, u32[]{:S(2)}, u32[]{:S(2)}) async-start(bf16[64,48,512]{2,1,0:T(8,128)(2,1)} %bitcast.2), calls=%async_computation.1 | async-start | bytes 6291456 | tf_op jit(solution)/shard_map/all_to_all | solution.py:98
  71.9 0.6 pad_maximum_fusion
  72.6 74.7 %all-to-all-done.1 = bf16[64,48,512]{2,1,0:T(8,128)(2,1)} async-done(((bf16[64,48,512]{2,1,0:T(8,128)(2,1)}), bf16[64,48,512]{2,1,0:T(8,128)(2,1)}, u32[]{:S(2)}, u32[]{:S(2)}) %all-to-all-start.1) | async-done | bytes 3145760 | tf_op jit(solution)/shard_map/all_to_all | solution.py:98
  147.3 4.6 %all-to-all-start.2 = ((bf16[64,48,512]{2,1,0:T(8,128)(2,1)}), bf16[64,48,512]{2,1,0:T(8,128)(2,1)S(1)}, u32[]{:S(2)}, u32[]{:S(2)}) async-start(bf16[64,48,512]{2,1,0:T(8,128)(2,1)} %all-to-all-done.1), calls=%async_computation.2 | async-start | bytes 6291456 | tf_op jit(solution)/shard_map/all_to_all | solution.py:97
  151.8 34.6 %all-to-all-done.2 = bf16[64,48,512]{2,1,0:T(8,128)(2,1)S(1)} async-done(((bf16[64,48,512]{2,1,0:T(8,128)(2,1)}), bf16[64,48,512]{2,1,0:T(8,128)(2,1)S(1)}, u32[]{:S(2)}, u32[]{:S(2)}) %all-to-all-start.2) | async-done | bytes 3145760 | tf_op jit(solution)/shard_map/all_to_all | solution.py:97
  186.4 2.6 copy.54
  189.1 1.0 copy.62
  190.1 4.6 %fusion.10 = f32[768,512]{1,0:T(8,128)} fusion(bf16[768,2048]{1,0:T(8,128)(2,1)S(1)} %bitcast.70, bf16[1,2048,512]{2,1,0:T(8,128)(2,1)} %all-gather.10.cloned.1.call-done), kind=kOutput, calls=%fused_computation.12 | convolution fusion | flops 1610612736 | bytes 6815744 | tf_op jit(solution)/shard_map/dot_general | solution.py:105
  194.8 8.0 %convolution_convert_fusion = bf16[768,2048]{1,0:T(8,128)(2,1)} fusion(bf16[1,512,2048]{2,1,0:T(8,128)(2,1)} %all-gather.14.cloned.1.call-done, f32[768,512]{1,0:T(8,128)} %fusion.10, bf16[768,2048]{1,0:T(8,128)(2,1)S(1)} %bitcast.71, bf16[1,2048,512]{2,1,0:T(8,128)(2,1)} %all-gather.12.cloned.1.call-done), kind=kOutput, calls=%fused_computation.6 | convolution fusion | flops 3225157632 | bytes 12058624 | tf_op jit(solution)/shard_map/dot_general | solution.py:108
  202.7 0.4 broadcast_in_dim.8
  203.1 1.5 copy-done.2
  204.6 1.5 constant_dynamic-slice_fusion
  206.1 1.5 collective-permute-start
  207.7 1.9 collective-permute-start.2
  209.6 6.9 %all-to-all-start.4 = ((bf16[4,192,512]{2,1,0:T(8,128)(2,1)}), bf16[4,192,512]{2,1,0:T(8,128)(2,1)}, u32[]{:S(2)}, u32[]{:S(2)}) async-start(bf16[4,192,512]{2,1,0:T(8,128)(2,1)} %bitcast.68), calls=%async_computation.4 | async-start | bytes 1572864 | tf_op jit(solution)/shard_map/all_to_all | solution.py:115
  216.5 10.4 %collective-permute-done = bf16[16,48,512]{2,1,0:T(8,128)(2,1)} collective-permute-done((bf16[16,48,512]{2,1,0:T(8,128)(2,1)}, bf16[16,48,512]{2,1,0:T(8,128)(2,1)}, u32[]{:S(2)}, u32[]{:S(2)}) %collective-permute-start) | collective-permute-done | bytes 786464 | tf_op jit(solution)/shard_map/ppermute | solution.py:68
  226.9 1.2 constant_dynamic-update-slice_fusion.1
  228.1 15.2 %collective-permute-done.1 = bf16[16,48,512]{2,1,0:T(8,128)(2,1)} collective-permute-done((bf16[16,48,512]{2,1,0:T(8,128)(2,1)}, bf16[16,48,512]{2,1,0:T(8,128)(2,1)}, u32[]{:S(2)}, u32[]{:S(2)}) %collective-permute-start.1) | collective-permute-done | bytes 786464 | tf_op jit(solution)/shard_map/ppermute | solution.py:68
  243.3 1.2 constant_dynamic-update-slice_fusion
  244.5 1.1 collective-permute-done.2
  245.6 1.2 constant_dynamic-update-slice_fusion.2
  246.8 1.7 copy-done
  248.5 1.3 all-to-all-done.4
  249.8 9.6 %all-to-all-start.3 = ((bf16[64,48,512]{2,1,0:T(8,128)(2,1)}), bf16[64,48,512]{2,1,0:T(8,128)(2,1)S(1)}, u32[]{:S(2)}, u32[]{:S(2)}) async-start(bf16[64,48,512]{2,1,0:T(8,128)(2,1)} %copy-done), calls=%async_computation.3 | async-start | bytes 6291456 | tf_op jit(solution)/shard_map/all_to_all | solution.py:33
  259.4 2.1 copy.60
  261.5 7.0 %fusion.4 = bf16[192,2048]{1,0:T(8,128)(2,1)} fusion(bf16[2048,2048]{1,0:T(8,128)(2,1)} %all-gather.8.cloned.1.call-done, bf16[192,2048]{1,0:T(8,128)(2,1)} %bitcast.74), kind=kOutput, calls=%fused_computation.8 | convolution fusion | flops 1611988992 | bytes 9961472 | tf_op jit(solution)/shard_map/dot_general | solution.py:121
  268.5 2.1 copy.65
  270.6 62.4 %all-to-all-done.3 = bf16[64,48,512]{2,1,0:T(8,128)(2,1)S(1)} async-done(((bf16[64,48,512]{2,1,0:T(8,128)(2,1)}), bf16[64,48,512]{2,1,0:T(8,128)(2,1)S(1)}, u32[]{:S(2)}, u32[]{:S(2)}) %all-to-all-start.3) | async-done | bytes 3145760 | tf_op jit(solution)/shard_map/all_to_all | solution.py:33
  333.0 8.4 %all-to-all-start.5 = ((bf16[192,4,512]{2,0,1:T(8,128)(2,1)}), bf16[192,4,512]{2,0,1:T(8,128)(2,1)}, u32[]{:S(2)}, u32[]{:S(2)}) async-start(bf16[192,4,512]{2,0,1:T(8,128)(2,1)} %bitcast.72), calls=%async_computation.5 | async-start | bytes 1572864 | tf_op jit(solution)/shard_map/all_to_all | solution.py:124
  341.4 0.6 add_divide_fusion
  342.2 5.4 %gather_fusion = bf16[1536,512]{1,0:T(8,128)(2,1)} fusion(bf16[3072,512]{1,0:T(8,128)(2,1)S(1)} %bitcast.65, s32[2048]{0:T(1024)S(1)} %pad_clamp_fusion), kind=kCustom, calls=%fused_computation | custom fusion | bytes 3151872 | tf_op jit(solution)/shard_map/gather | solution.py:111
  347.6 3.4 reshape.96
  351.1 5.9 %multiply_reduce_fusion = f32[768,512]{1,0:T(8,128)} fusion(f32[768,2,512]{2,1,0:T(2,128)S(1)} %reshape.96, f32[768,2]{1,0:T(8,128)S(1)} %copy.55), kind=kLoop, calls=%fused_computation.7 | loop fusion | flops 1179648 | bytes 4724736 | tf_op jit(solution)/shard_map/reduce_sum | solution.py:114
  357.0 2.7 fusion.16
  (50 shorter events, 2.3 us)
Async XLA Ops:
  6.5 2.2 copy-start.3
  6.5 8.5 %copy-start.4 = (s32[768,2]{0,1:T(2,128)S(1)}, s32[768,2]{0,1:T(2,128)}, u32[]{:S(2)}) copy-start(s32[768,2]{0,1:T(2,128)} %param.12) | copy-start | bytes 18436
  6.5 183.6 %all-gather.10.cloned.1.call-start = ((), (), s32[]{:S(2)}) async-start(), calls=%async_computation.7 | async-start | bytes 2621440 | tf_op jit(solution)/shard_map/all_gather | solution.py:93
  7.3 187.5 %all-gather.14.cloned.1.call-start = ((), (), s32[]{:S(2)}) async-start(), calls=%async_computation.9 | async-start | bytes 2621440 | tf_op jit(solution)/shard_map/all_gather | solution.py:95
  8.0 186.8 %all-gather.12.cloned.1.call-start = ((), (), s32[]{:S(2)}) async-start(), calls=%async_computation.8 | async-start | bytes 2621440 | tf_op jit(solution)/shard_map/all_gather | solution.py:94
  9.6 38.5 %all-to-all-start = ((f32[4,1,768]{2,1,0:T(1,128)}), f32[4,1,768]{2,1,0:T(1,128)S(1)}, u32[]{:S(2)}, u32[]{:S(2)}) async-start(f32[4,1,768]{2,1,0:T(1,128)} %broadcast_in_dim.10), calls=%async_computation | async-start | bytes 24576 | tf_op jit(solution)/shard_map/all_to_all | solution.py:12
  15.7 19.3 %copy-start.5 = (bf16[256,32]{0,1:T(8,128)(2,1)S(1)}, bf16[256,32]{0,1:T(8,128)(2,1)}, u32[]{:S(2)}) copy-start(bf16[256,32]{0,1:T(8,128)(2,1)} %param.18) | copy-start | bytes 49156
  15.7 19.3 %copy-start.6 = (bf16[32,256]{1,0:T(8,128)(2,1)S(1)}, bf16[32,256]{1,0:T(8,128)(2,1)}, u32[]{:S(2)}) copy-start(bf16[32,256]{1,0:T(8,128)(2,1)} %param.17) | copy-start | bytes 49156
  16.2 31.9 %copy-start.9 = (f32[512]{0:T(512)S(1)}, f32[512]{0:T(512)}, u32[]{:S(2)}) copy-start(f32[512]{0:T(512)} %param.11) | copy-start | bytes 6148
  48.4 0.9 copy-start.1
  60.2 87.0 %all-to-all-start.1 = ((bf16[64,48,512]{2,1,0:T(8,128)(2,1)}), bf16[64,48,512]{2,1,0:T(8,128)(2,1)}, u32[]{:S(2)}, u32[]{:S(2)}) async-start(bf16[64,48,512]{2,1,0:T(8,128)(2,1)} %bitcast.2), calls=%async_computation.1 | async-start | bytes 6291456 | tf_op jit(solution)/shard_map/all_to_all | solution.py:98
  71.8 189.7 %all-gather.8.cloned.1.call-start = ((), (), s32[]{:S(2)}) async-start(), calls=%async_computation.6 | async-start | bytes 8519680 | tf_op jit(solution)/shard_map/all_gather | solution.py:24
  147.3 39.2 %all-to-all-start.2 = ((bf16[64,48,512]{2,1,0:T(8,128)(2,1)}), bf16[64,48,512]{2,1,0:T(8,128)(2,1)S(1)}, u32[]{:S(2)}, u32[]{:S(2)}) async-start(bf16[64,48,512]{2,1,0:T(8,128)(2,1)} %all-to-all-done.1), calls=%async_computation.2 | async-start | bytes 6291456 | tf_op jit(solution)/shard_map/all_to_all | solution.py:97
  202.7 1.9 copy-start.2
  206.1 20.7 %collective-permute-start = (bf16[16,48,512]{2,1,0:T(8,128)(2,1)}, bf16[16,48,512]{2,1,0:T(8,128)(2,1)}, u32[]{:S(2)}, u32[]{:S(2)}) collective-permute-start(bf16[16,48,512]{2,1,0:T(8,128)(2,1)} %get-tuple-element.7), channel_id=1, source_target_pairs={{0,1},{1,0},{2,3},{3,2},{4,5},{5,4},{6,7},{7,6},{8,9},{9,8},{10,11... | collective-permute-start | bytes 2359304 | tf_op jit(solution)/shard_map/ppermute | solution.py:68
  207.6 35.7 %collective-permute-start.1 = (bf16[16,48,512]{2,1,0:T(8,128)(2,1)}, bf16[16,48,512]{2,1,0:T(8,128)(2,1)}, u32[]{:S(2)}, u32[]{:S(2)}) collective-permute-start(bf16[16,48,512]{2,1,0:T(8,128)(2,1)} %get-tuple-element.6), channel_id=1, source_target_pairs={{0,2},{1,3},{2,0},{3,1},{4,6},{5,7},{6,4},{7,5},{8,10},{9,11},{10,... | collective-permute-start | bytes 2359304 | tf_op jit(solution)/shard_map/ppermute | solution.py:68
  207.7 37.9 %collective-permute-start.2 = (bf16[16,48,512]{2,1,0:T(8,128)(2,1)}, bf16[16,48,512]{2,1,0:T(8,128)(2,1)}, u32[]{:S(2)}, u32[]{:S(2)}) collective-permute-start(bf16[16,48,512]{2,1,0:T(8,128)(2,1)} %get-tuple-element.5), channel_id=1, source_target_pairs={{0,3},{1,2},{2,1},{3,0},{4,7},{5,6},{6,5},{7,4},{8,11},{9,10},{10,... | collective-permute-start | bytes 2359304 | tf_op jit(solution)/shard_map/ppermute | solution.py:68
  209.6 40.2 %all-to-all-start.4 = ((bf16[4,192,512]{2,1,0:T(8,128)(2,1)}), bf16[4,192,512]{2,1,0:T(8,128)(2,1)}, u32[]{:S(2)}, u32[]{:S(2)}) async-start(bf16[4,192,512]{2,1,0:T(8,128)(2,1)} %bitcast.68), calls=%async_computation.4 | async-start | bytes 1572864 | tf_op jit(solution)/shard_map/all_to_all | solution.py:115
  246.8 1.7 copy-start
  249.8 83.3 %all-to-all-start.3 = ((bf16[64,48,512]{2,1,0:T(8,128)(2,1)}), bf16[64,48,512]{2,1,0:T(8,128)(2,1)S(1)}, u32[]{:S(2)}, u32[]{:S(2)}) async-start(bf16[64,48,512]{2,1,0:T(8,128)(2,1)} %copy-done), calls=%async_computation.3 | async-start | bytes 6291456 | tf_op jit(solution)/shard_map/all_to_all | solution.py:33
  268.5 72.9 %copy-start.10 = (f32[512]{0:T(512)S(1)}, f32[512]{0:T(512)}, u32[]{:S(2)}) copy-start(f32[512]{0:T(512)} %param.19) | copy-start | bytes 6148
  268.5 73.5 %copy-start.8 = (f32[768,2]{0,1:T(2,128)S(1)}, f32[768,2]{0,1:T(2,128)}, u32[]{:S(2)}) copy-start(f32[768,2]{0,1:T(2,128)} %param.13) | copy-start | bytes 18436
  333.0 24.0 %all-to-all-start.5 = ((bf16[192,4,512]{2,0,1:T(8,128)(2,1)}), bf16[192,4,512]{2,0,1:T(8,128)(2,1)}, u32[]{:S(2)}, u32[]{:S(2)}) async-start(bf16[192,4,512]{2,0,1:T(8,128)(2,1)} %bitcast.72), calls=%async_computation.5 | async-start | bytes 1572864 | tf_op jit(solution)/shard_map/all_to_all | solution.py:124
  351.1 5.9 %copy-start.7 = (f32[512]{0:T(512)S(1)}, f32[512]{0:T(512)}, u32[]{:S(2)}) copy-start(f32[512]{0:T(512)} %add_divide_fusion) | copy-start | bytes 6148
Sparse Core Ops, SparseCore 0:
  9.1 36.2 all-gather.9
  47.2 33.0 all-gather.13
  82.1 33.3 all-gather.11
  118.1 84.6 all-gather.7
